TPU v7x, 32 devices: a whole 2x2x4 slice. The times are simulated.
32 devices in a mesh: rep: 2 (over y), fs: 4 (over z), tp: 4 (over x, core).
Axes of the slice: x: 2, y: 2, z: 4, core: 2. Of those that a mesh axis runs over, the one named last changes fastest.
Arguments:
- gate_pre: bfloat16 [8192, 3072], P(('rep', 'fs'), 'tp'), may hold values from -6 to 6
- up_pre: bfloat16 [8192, 3072], P(('rep', 'fs'), 'tp'), may hold values from -6 to 6
- out_grad: bfloat16 [8192, 2048], P(('rep', 'fs')), may hold values from -8 to 8
- w_down: bfloat16 [3072, 2048], P('tp', 'fs'), may hold values from -0.109375 to 0.109375
Outputs:
- d_gate: bfloat16 [8192, 3072], P(('rep', 'fs'), 'tp')
- d_up: bfloat16 [8192, 3072], P(('rep', 'fs'), 'tp')
- grad_down: float32 [3072, 2048], P('tp', 'fs')
- row_energy: float32 [3072], P('tp')
All inputs are finite; a program needn't handle non-finite values.
Results may differ from a plain program's by a relative error of at most 0.0034.
Values may be sent and summed in bfloat16 or wider, within the bound.
A program may use at most 64 MiB of HBM per device.

v0:
```python
import functools

import jax
import jax.numpy as jnp
from jax import lax
from jax.experimental import pallas as pl
from jax.experimental.pallas import tpu as pltpu
from jax.sharding import PartitionSpec as P

MESH = pl.DeviceIdType.MESH
F32 = jnp.float32
BF16 = jnp.bfloat16
PIECES = 6
SPLIT = 2
LAG = 2
VMEM_LIMIT = 52 * 1024 * 1024


def plain(gate_pre, up_pre, out_grad, w_down):
    gate_f = gate_pre.astype(F32)
    up_f = up_pre.astype(F32)
    sig = jax.nn.sigmoid(gate_f)
    act = gate_f * sig
    hidden = (act * up_f).astype(BF16)
    tokens_all = out_grad.shape[0] * lax.axis_size("rep") * lax.axis_size("fs")
    factor = float(tokens_all) ** (-0.5)
    weight_whole = lax.all_gather(w_down, "fs", axis=1, tiled=True)
    dhid = lax.dot_general(out_grad, weight_whole, (((1,), (1,)), ((), ())), preferred_element_type=F32)
    d_up = (dhid * act).astype(BF16)
    d_gate = (dhid * up_f * sig * (1.0 + gate_f * (1.0 - sig))).astype(BF16)
    shard = lax.psum_scatter(
        lax.dot_general(out_grad, hidden, (((0,), (0,)), ((), ())), preferred_element_type=F32),
        "fs",
        scatter_dimension=0,
        tiled=True,
    )
    shard = lax.psum(shard, "rep")
    grad_down = shard.T * factor
    energy = lax.psum(jnp.sum(grad_down * grad_down, axis=1), "fs") / out_grad.shape[1]
    return (d_gate, d_up, grad_down, energy)


def kernel(
    n, factor, width,
    g_hbm, u_hbm, og_hbm, w_hbm,
    dg, du, gd, en_ref,
    g, u, og, w, hid, part, zsend, zrecv, ysend, yrecv, fsend, frecv, lanes, esend, erecv,
    in_sem, zs_sem, zr_sem, as_sem, ar_sem, ys_sem, yr_sem, fs_sem, fr_sem, es_sem, er_sem,
):
    rep = lax.axis_index("rep")
    k = lax.axis_index("fs")
    mate = 1 - rep
    cols = w.shape[3]
    hidden_units = g.shape[1]
    tokens = g.shape[0]
    count = PIECES - SPLIT

    def piece(c):
        return c + jnp.where(c < SPLIT, rep * SPLIT, SPLIT)

    def loop(lo, hi, body):
        lax.fori_loop(lo, hi, lambda i, x: (body(i), x)[1], 0)

    in_w = pltpu.make_async_copy(w_hbm, w.at[k], in_sem.at[0])
    in_g = pltpu.make_async_copy(g_hbm, g, in_sem.at[1])
    in_u = pltpu.make_async_copy(u_hbm, u, in_sem.at[2])
    in_og = [
        pltpu.make_async_copy(og_hbm.at[:, pl.ds(j * cols, cols)], og.at[j], in_sem.at[3 + j]) for j in range(n)
    ]
    in_w.start()
    in_g.start()
    in_u.start()
    for j in range(n):
        in_og[j].start()

    barrier = pltpu.get_barrier_semaphore()
    for t in range(1, n):
        pl.semaphore_signal(barrier, inc=1, device_id={"fs": lax.rem(k + t, n)}, device_id_type=MESH)
    pl.semaphore_signal(barrier, inc=1, device_id={"rep": mate}, device_id_type=MESH)
    pl.semaphore_wait(barrier, n)
    in_w.wait()

    at = (k, n - 1 - k)
    sign = (1, -1)

    def along(d, s, c, src, dst):
        return pltpu.make_async_remote_copy(
            src_ref=src, dst_ref=dst, send_sem=zs_sem.at[d, s, c], recv_sem=zr_sem.at[d, s, c],
            device_id={"fs": k + sign[d]}, device_id_type=MESH,
        )

    def across(src, dst, send, recv):
        return pltpu.make_async_remote_copy(
            src_ref=src, dst_ref=dst, send_sem=send, recv_sem=recv,
            device_id={"rep": mate}, device_id_type=MESH,
        )

    def first(c):
        for d in range(2):

            @pl.when(at[d] < n - 1)
            def _():
                block = w.at[k, piece(c)]
                along(d, 0, c, block, block).start()

    loop(0, count, first)

    in_g.wait()
    in_u.wait()
    rows = tokens // 8

    def make_hidden(i):
        at_rows = pl.ds(pl.multiple_of(i * rows, rows), rows)
        gate = g[at_rows, :].astype(F32)
        act = gate * jax.nn.sigmoid(gate)
        h = (act * u[at_rows, :].astype(F32)).astype(BF16)
        hid[:, at_rows] = h.T

    loop(0, 8, make_hidden)
    for j in range(n):
        in_og[j].wait()

    def make_part(i):
        j = jnp.where(i % 2 == 0, n - 1 - i // 2, i // 2)
        part[j] = jnp.dot(hid[...], og[j], preferred_element_type=F32).reshape(part.shape[1:])
        ysend[j] = part[j, pl.ds(mate * SPLIT, SPLIT)].astype(BF16)
        across(ysend.at[j], yrecv.at[j], ys_sem.at[j], yr_sem.at[j]).start()

    loop(0, n, make_part)

    def pass_on(s, c):
        p = piece(c)
        for d in range(2):
            place = at[d]

            @pl.when(place > 0)
            def _():
                along(d, s - 1, c, zsend.at[d, 0, c], zrecv.at[d, 0, c]).wait_recv()

            @pl.when(s <= place)
            def _():
                block = w.at[k - sign[d] * s, p]

                @pl.when(place < n - 1)
                def _():
                    along(d, s, c, block, block).start()

                @pl.when(c < SPLIT)
                def _():
                    j = k - sign[d] * s
                    across(block, block, as_sem.at[j, c], ar_sem.at[j, c]).start()

            @pl.when(s > place)
            def _():
                j = k + sign[d] * (n - s)

                @pl.when(c == 0)
                def _():
                    across(ysend.at[j], yrecv.at[j], ys_sem.at[j], yr_sem.at[j]).wait_recv()

                @pl.when(c < SPLIT)
                def _():
                    part[j, p] += yrecv[j, jnp.minimum(c, SPLIT - 1)].astype(F32)

                if s > 1:

                    @pl.when(place > 0)
                    def _():
                        part[j, p] += zrecv[d, s - 2, c].astype(F32)

                zsend[d, s - 1, c] = part[j, p].astype(BF16)
                along(d, s, c, zsend.at[d, s - 1, c], zrecv.at[d, s - 1, c]).start()

    for s in range(1, n):
        loop(0, count, functools.partial(pass_on, s))

    def finish(c):
        p = piece(c)

        @pl.when(c == 0)
        def _():
            across(ysend.at[k], yrecv.at[k], ys_sem.at[k], yr_sem.at[k]).wait_recv()

        @pl.when(c < SPLIT)
        def _():
            part[k, p] += yrecv[k, jnp.minimum(c, SPLIT - 1)].astype(F32)

        for d in range(2):

            @pl.when(at[d] > 0)
            def _():
                along(d, n - 1, c, zsend.at[d, n - 2, c], zrecv.at[d, n - 2, c]).wait_recv()
                part[k, p] += zrecv[d, n - 2, c].astype(F32)

        fsend[c] = part[k, p].astype(BF16)
        across(fsend.at[c], frecv.at[c], fs_sem.at[c], fr_sem.at[c]).start()

    def put(p, value):
        gd[p] = value
        sq = value * value
        total = sq[:, :128]
        for b in range(1, cols // 128):
            total += sq[:, b * 128 : (b + 1) * 128]
        lanes[p] = total

    def deliver(c):
        across(fsend.at[c], frecv.at[c], fs_sem.at[c], fr_sem.at[c]).wait_recv()

        @pl.when(c < SPLIT)
        def _():
            put(rep * SPLIT + c, fsend[c].astype(F32) * factor)
            put(mate * SPLIT + c, frecv[c].astype(F32) * factor)

        @pl.when(c >= SPLIT)
        def _():
            put(c + SPLIT, (fsend[c].astype(F32) + frecv[c].astype(F32)) * factor)

    blocks = 4
    brows = tokens // blocks

    def activations(i):
        at_rows = pl.ds(pl.multiple_of(i * brows, brows), brows)
        dhid = jnp.zeros((brows, hidden_units), F32)
        for j in range(n):
            dhid += lax.dot_general(
                og[j, at_rows, :], w[j].reshape(hidden_units, cols), (((1,), (1,)), ((), ())),
                preferred_element_type=F32,
            )
        gate = g[at_rows, :].astype(F32)
        up = u[at_rows, :].astype(F32)
        sig = jax.nn.sigmoid(gate)
        du[at_rows, :] = (dhid * (gate * sig)).astype(BF16)
        dg[at_rows, :] = (dhid * up * sig * (1.0 + gate * (1.0 - sig))).astype(BF16)

    def gathered(j):
        @pl.when(j != k)
        def _():
            for c in range(SPLIT):
                block = w.at[j, mate * SPLIT + c]
                across(block, block, as_sem.at[j, c], ar_sem.at[j, c]).wait_recv()

    def last(c):
        @pl.when(c < count)
        def _():
            finish(c)

        @pl.when(c == 0)
        def _():
            loop(0, n, gathered)

        @pl.when(c < blocks)
        def _():
            activations(c)

        @pl.when(c >= LAG)
        def _():
            deliver(c - LAG)

    loop(0, count + LAG, last)

    row = jnp.sum(lanes[...].reshape(hidden_units, 128).T, axis=0, keepdims=True)
    esend[...] = jnp.broadcast_to(row, esend.shape)

    def energy_copy(to, slot):
        return pltpu.make_async_remote_copy(
            src_ref=esend, dst_ref=erecv.at[slot], send_sem=es_sem.at[to], recv_sem=er_sem.at[slot],
            device_id={"fs": to}, device_id_type=MESH,
        )

    for t in range(1, n):
        energy_copy(lax.rem(k + t, n), k).start()

    def sent(c):
        for d in range(2):

            @pl.when(at[d] < n - 1)
            def _():
                for s in range(n):
                    along(d, s, c, zsend.at[d, 0, c], zrecv.at[d, 0, c]).wait_send()

        across(fsend.at[c], frecv.at[c], fs_sem.at[c], fr_sem.at[c]).wait_send()

    loop(0, count, sent)

    def sent_across(j):
        across(ysend.at[j], yrecv.at[j], ys_sem.at[j], yr_sem.at[j]).wait_send()

        @pl.when(j != k)
        def _():
            for c in range(SPLIT):
                block = w.at[j, rep * SPLIT + c]
                across(block, block, as_sem.at[j, c], ar_sem.at[j, c]).wait_send()

    loop(0, n, sent_across)

    for t in range(1, n):
        energy_copy(k, lax.rem(k + t, n)).wait_recv()
    total = jnp.zeros((8, hidden_units), F32)
    for j in range(n):
        total += jnp.where(j == k, esend[...], erecv[j])
    en_ref[...] = total[:1] * (1.0 / width)
    for t in range(1, n):
        energy_copy(lax.rem(k + t, n), k).wait_send()


def write_out(dg, du, gd, en, dg_hbm, du_hbm, gd_hbm, en_out, sem):
    copies = [
        pltpu.make_async_copy(src, dst, sem.at[i])
        for i, (src, dst) in enumerate(((dg, dg_hbm), (du, du_hbm), (gd, gd_hbm)))
    ]
    for copy in copies:
        copy.start()
    en_out[...] = en[0, :]
    for copy in copies:
        copy.wait()


def fused(n, gate_pre, up_pre, out_grad, w_down):
    tokens, units = gate_pre.shape
    width = out_grad.shape[1]
    cols = w_down.shape[1]
    rows = units // PIECES
    count = PIECES - SPLIT
    factor = float(tokens * lax.axis_size("rep") * n) ** (-0.5)
    any_spec = pl.BlockSpec(memory_space=pl.ANY)
    vmem_spec = pl.BlockSpec(memory_space=pltpu.VMEM)
    dma = pltpu.SemaphoreType.DMA
    d_gate, d_up, grad, energy = pl.pallas_call(
        functools.partial(kernel, n, factor, width),
        out_shape=(
            pltpu.VMEM((tokens, units), BF16),
            pltpu.VMEM((tokens, units), BF16),
            pltpu.VMEM((PIECES, rows, cols), F32),
            pltpu.VMEM((1, units), F32),
        ),
        in_specs=[any_spec] * 4,
        out_specs=(vmem_spec,) * 4,
        scratch_shapes=[
            pltpu.VMEM((tokens, units), BF16),
            pltpu.VMEM((tokens, units), BF16),
            pltpu.VMEM((n, tokens, cols), BF16),
            pltpu.VMEM((n, PIECES, rows, cols), BF16),
            pltpu.VMEM((units, tokens), BF16),
            pltpu.VMEM((n, PIECES, rows, cols), F32),
            pltpu.VMEM((2, n - 1, count, rows, cols), BF16),
            pltpu.VMEM((2, n - 1, count, rows, cols), BF16),
            pltpu.VMEM((n, SPLIT, rows, cols), BF16),
            pltpu.VMEM((n, SPLIT, rows, cols), BF16),
            pltpu.VMEM((count, rows, cols), BF16),
            pltpu.VMEM((count, rows, cols), BF16),
            pltpu.VMEM((PIECES, rows, 128), F32),
            pltpu.VMEM((8, units), F32),
            pltpu.VMEM((n, 8, units), F32),
            dma((3 + n,)),
            dma((2, n, count)),
            dma((2, n, count)),
            dma((n, SPLIT)),
            dma((n, SPLIT)),
            dma((n,)),
            dma((n,)),
            dma((count,)),
            dma((count,)),
            dma((n,)),
            dma((n,)),
        ],
        compiler_params=pltpu.CompilerParams(
            collective_id=0, has_side_effects=True, vmem_limit_bytes=VMEM_LIMIT
        ),
    )(gate_pre, up_pre, out_grad, w_down.reshape(PIECES, rows, cols))
    return pl.pallas_call(
        write_out,
        out_shape=(
            jax.ShapeDtypeStruct((tokens, units), BF16),
            jax.ShapeDtypeStruct((tokens, units), BF16),
            jax.ShapeDtypeStruct((units, cols), F32),
            jax.ShapeDtypeStruct((units,), F32),
        ),
        in_specs=[vmem_spec] * 4,
        out_specs=(any_spec, any_spec, any_spec, vmem_spec),
        scratch_shapes=[dma((3,))],
        compiler_params=pltpu.CompilerParams(vmem_limit_bytes=4 * 1024 * 1024),
    )(d_gate, d_up, grad.reshape(units, cols), energy)


def solution(mesh):
    reps, n = mesh.shape["rep"], mesh.shape["fs"]

    def local(gate_pre, up_pre, out_grad, w_down):
        units, cols = w_down.shape
        fits = reps == 2 and 2 <= n <= 4 and cols % 128 == 0 and units % (PIECES * 16) == 0 and units % 128 == 0
        if fits and gate_pre.shape[0] % 1024 == 0:
            return fused(n, gate_pre, up_pre, out_grad, w_down)
        return plain(gate_pre, up_pre, out_grad, w_down)

    placed = (P(("rep", "fs"), "tp"), P(("rep", "fs"), "tp"), P(("rep", "fs"), None), P("tp", "fs"))
    return jax.shard_map(
        local,
        mesh=mesh,
        in_specs=placed,
        out_specs=(P(("rep", "fs"), "tp"), P(("rep", "fs"), "tp"), P("tp", "fs"), P("tp")),
        check_vma=False,
    )
```

profile of v0, /device:TPU:0, one launch (start us, length us, event | category | flops | bytes accessed | tf_op | source)
XLA Modules:
  0.0 68.7 jit_solution(10482607929492747505)
XLA Ops:
  0.6 65.3 %shard_map.75 = (bf16[1024,768]{1,0:T(8,128)(2,1)S(1)}, bf16[1024,768]{1,0:T(8,128)(2,1)S(1)}, f32[6,128,512]{2,1,0:T(8,128)S(1)}, f32[1,768]{1,0:T(1,128)S(1)}) custom-call(bf16[1024,768]{1,0:T(8,128)(2,1)} %g_hbm.1, bf16[1024,768]{1,0:T(8,128)(2,1)} %u_hbm.1, bf16[1024,2048]{1,0:T(8,128)(2,1)} %og_hbm.1, bf16[6,128,512]{2,1,0:T(8,128)(2,1)} %bitcast.3), custom_call_target="tpu_custom_call" | custom-call | tf_op jit(solution)/shard_map/pallas_call | solution.py:328
  65.9 2.8 %shard_map.76 = (bf16[1024,768]{1,0:T(8,128)(2,1)}, bf16[1024,768]{1,0:T(8,128)(2,1)}, f32[768,512]{1,0:T(8,128)}, f32[768]{0:T(1024)}) custom-call(bf16[1024,768]{1,0:T(8,128)(2,1)S(1)} %get-tuple-element.8.dg, bf16[1024,768]{1,0:T(8,128)(2,1)S(1)} %get-tuple-element.9.du, f32[768,512]{1,0:T(8,128)S(1)} %bitcast.2, f32[1,768]{1,0:T(1,128)S(1)} %get-tuple-element.11.en), custom_call_target="tpu_custom_call" | custom-call | tf_op jit(solution)/shard_map/pallas_call | solution.py:370
where the time goes:
time: 68.8 us; the launch traced here: 68.7 us
  Pallas kernels  68 us (99%)
    pallas_call x1, Pallas kernels, fused(): pl.pallas_call(functools.partial(kernel, n, factor, width), out_shape=(pl...  65.3 us
    pallas_call x1, Pallas kernels, fused(): pl.pallas_call(write_out, out_shape=(jax.ShapeDtypeStruct((tokens, units)...  2.78 us

commit v1 on v0

v1 whole, which is shorter than its diff:
```python
import functools

import jax
import jax.numpy as jnp
from jax import lax
from jax.experimental import pallas as pl
from jax.experimental.pallas import tpu as pltpu
from jax.sharding import PartitionSpec as P

MESH = pl.DeviceIdType.MESH
F32 = jnp.float32
BF16 = jnp.bfloat16
PIECES = 24
SPLIT = 7
LAG = 2
LOADS = 4
BEFORE = 2
VMEM_LIMIT = 52 * 1024 * 1024


def plain(gate_pre, up_pre, out_grad, w_down):
    gate_f = gate_pre.astype(F32)
    up_f = up_pre.astype(F32)
    sig = jax.nn.sigmoid(gate_f)
    act = gate_f * sig
    hidden = (act * up_f).astype(BF16)
    tokens_all = out_grad.shape[0] * lax.axis_size("rep") * lax.axis_size("fs")
    factor = float(tokens_all) ** (-0.5)
    weight_whole = lax.all_gather(w_down, "fs", axis=1, tiled=True)
    dhid = lax.dot_general(out_grad, weight_whole, (((1,), (1,)), ((), ())), preferred_element_type=F32)
    d_up = (dhid * act).astype(BF16)
    d_gate = (dhid * up_f * sig * (1.0 + gate_f * (1.0 - sig))).astype(BF16)
    shard = lax.psum_scatter(
        lax.dot_general(out_grad, hidden, (((0,), (0,)), ((), ())), preferred_element_type=F32),
        "fs",
        scatter_dimension=0,
        tiled=True,
    )
    shard = lax.psum(shard, "rep")
    grad_down = shard.T * factor
    energy = lax.psum(jnp.sum(grad_down * grad_down, axis=1), "fs") / out_grad.shape[1]
    return (d_gate, d_up, grad_down, energy)


def kernel(
    n, factor, width,
    g_hbm, u_hbm, og_hbm, w_hbm,
    dg, du, gd, en_ref,
    g, u, og, w, hid, part, dhid, zsend, zrecv, ysend, yrecv, fsend, frecv,
    lanes_u, lanes_s, esu, eru, ess, ers,
    in_sem, og_sem, zs_sem, zr_sem, as_sem, ar_sem, ys_sem, yr_sem, fs_sem, fr_sem,
    us_sem, ur_sem, ss_sem, sr_sem,
):
    rep = lax.axis_index("rep")
    k = lax.axis_index("fs")
    mate = 1 - rep
    cols = w.shape[3]
    rows = w.shape[2]
    hidden_units = g.shape[1]
    tokens = g.shape[0]
    count = PIECES - SPLIT
    free = PIECES - 2 * SPLIT
    pairs = count // 2
    chunk = tokens // LOADS

    def piece(c):
        return c + jnp.where(c < free, 2 * SPLIT, rep * SPLIT - free)

    def loop(lo, hi, body):
        lax.fori_loop(lo, hi, lambda i, x: (body(i), x)[1], 0)

    def steps(lo, hi, body):
        loop(lo, min(hi, pairs), lambda i: body(2 * i, 2, i))
        if hi > pairs:
            body(k * 0 + 2 * pairs, 1, k * 0 + pairs)

    end = pairs + count % 2
    low = jnp.minimum(k, n - 1 - k)

    def chosen(i):
        far = jnp.where(i < n - 1 - low, n - 1 - i, jnp.where(i < n - 1, i - (n - 1 - low), low))
        return jnp.where(2 * k >= n, n - 1 - far, far)

    def rows_at(i):
        return pl.ds(pl.multiple_of(i * chunk, chunk), chunk)

    def in_g(i):
        return pltpu.make_async_copy(g_hbm.at[rows_at(i)], g.at[rows_at(i)], in_sem.at[1 + i])

    def in_u(i):
        return pltpu.make_async_copy(u_hbm.at[rows_at(i)], u.at[rows_at(i)], in_sem.at[1 + LOADS + i])

    def in_og(j):
        part_of = pl.ds(pl.multiple_of(j * cols, cols), cols)
        return pltpu.make_async_copy(og_hbm.at[:, part_of], og.at[j], og_sem.at[j])

    at = (k, n - 1 - k)
    sign = (1, -1)

    barrier = pltpu.get_barrier_semaphore()
    for d in range(2):

        @pl.when(at[d] < n - 1)
        def _():
            pl.semaphore_signal(barrier, inc=1, device_id={"fs": k + sign[d]}, device_id_type=MESH)

    pl.semaphore_signal(barrier, inc=1, device_id={"rep": mate}, device_id_type=MESH)
    in_w = pltpu.make_async_copy(w_hbm, w.at[k], in_sem.at[0])
    in_w.start()

    def load(i):
        in_g(i).start()
        in_u(i).start()

    loop(0, LOADS, load)
    loop(0, n, lambda i: in_og(chosen(i)).start())
    lanes_u[...] = jnp.zeros_like(lanes_u)
    lanes_s[...] = jnp.zeros_like(lanes_s)
    def along(d, s, i, src, dst):
        return pltpu.make_async_remote_copy(
            src_ref=src, dst_ref=dst, send_sem=zs_sem.at[d, s], recv_sem=zr_sem.at[d, s, i],
            device_id={"fs": k + sign[d]}, device_id_type=MESH,
        )

    def across(src, dst, send, recv):
        return pltpu.make_async_remote_copy(
            src_ref=src, dst_ref=dst, send_sem=send, recv_sem=recv,
            device_id={"rep": mate}, device_id_type=MESH,
        )

    def early(j):
        return across(ysend.at[j], yrecv.at[j], ys_sem.at[0], yr_sem.at[j])

    def final(c, m, i):
        return across(fsend.at[pl.ds(c, m)], frecv.at[pl.ds(c, m)], fs_sem.at[0], fr_sem.at[i])

    def crossing(j, owner, start, m):
        block = w.at[j, pl.ds(owner * SPLIT + start, m)]
        return across(block, block, as_sem.at[j], ar_sem.at[j])

    def make_hidden(i):
        in_g(i).wait()
        in_u(i).wait()
        gate = g[rows_at(i), :].astype(F32)
        act = gate * jax.nn.sigmoid(gate)
        h = (act * u[rows_at(i), :].astype(F32)).astype(BF16)
        hid[:, rows_at(i)] = h.T

    loop(0, BEFORE, make_hidden)
    pl.semaphore_wait(barrier, 1 + (k > 0).astype(jnp.int32) + (k < n - 1).astype(jnp.int32))
    in_w.wait()

    def first(c, m, i):
        for d in range(2):

            @pl.when(at[d] < n - 1)
            def _():
                block = w.at[k, pl.ds(piece(c), m)]
                along(d, 0, i, block, block).start()

    steps(0, end, first)
    loop(BEFORE, LOADS, make_hidden)

    def product(j, start, pieces):
        some = hid[pl.ds(pl.multiple_of(start * rows, rows), pieces * rows), :]
        return jnp.dot(some, og[j], preferred_element_type=F32).reshape(pieces, rows, cols)

    def make_part(i):
        j = chosen(i)
        in_og(j).wait()
        ysend[j] = product(j, mate * SPLIT, SPLIT).astype(BF16)
        early(j).start()
        part[j, pl.ds(2 * SPLIT, free)] = product(j, 2 * SPLIT, free)
        part[j, pl.ds(rep * SPLIT, SPLIT)] = product(j, rep * SPLIT, SPLIT)

    loop(0, n, make_part)

    def multiply(j, at_rows):
        return lax.dot_general(
            og[j, at_rows, :], w[j].reshape(hidden_units, cols), (((1,), (1,)), ((), ())),
            preferred_element_type=F32,
        )

    def own(i):
        at_rows = pl.ds(pl.multiple_of(i * 256, 256), 256)
        dhid[at_rows, :] = multiply(k, at_rows)

    loop(0, tokens // 256, own)

    def pass_on(s, c, m, i):
        p = piece(c)
        for d in range(2):
            place = at[d]
            some = pl.ds(c, m)

            @pl.when(place > 0)
            def _():
                along(d, s - 1, i, zsend.at[d, 0, some], zrecv.at[d, 0, some]).wait_recv()

            @pl.when(s <= place)
            def _():
                j = k - sign[d] * s
                block = w.at[j, pl.ds(p, m)]

                @pl.when(place < n - 1)
                def _():
                    along(d, s, i, block, block).start()

                @pl.when(c >= free)
                def _():
                    crossing(j, rep, c - free, m).start()

            @pl.when(s > place)
            def _():
                j = k + sign[d] * (n - s)

                @pl.when(c == free)
                def _():
                    early(j).wait_recv()

                @pl.when(c >= free)
                def _():
                    part[j, pl.ds(p, m)] += yrecv[j, pl.ds(jnp.maximum(c - free, 0), m)].astype(F32)

                if s > 1:

                    @pl.when(place > 0)
                    def _():
                        part[j, pl.ds(p, m)] += zrecv[d, s - 2, some].astype(F32)

                zsend[d, s - 1, some] = part[j, pl.ds(p, m)].astype(BF16)
                along(d, s, i, zsend.at[d, s - 1, some], zrecv.at[d, s - 1, some]).start()

    def gathered(j):
        crossing(j, mate, 0, SPLIT).wait_recv()

    halves = 2
    half = tokens // halves

    def gather(far, part_of):
        at_rows = pl.ds(pl.multiple_of(part_of * half, half), half)
        for d in range(2):

            @pl.when(at[d] >= far)
            def _():
                j = k - sign[d] * far

                @pl.when(part_of == 0)
                def _():
                    gathered(j)

                dhid[at_rows, :] += multiply(j, at_rows)

    for s in range(1, n - 1):
        steps(0, end, functools.partial(pass_on, s))
    steps(0, pairs - 2, functools.partial(pass_on, n - 1))
    loop(0, halves, functools.partial(gather, 1))
    steps(pairs - 2, end, functools.partial(pass_on, n - 1))

    def put(p, m, value, lanes):
        gd[pl.ds(p, m)] = value
        if lanes is not None:
            sq = value * value
            total = sq[:, :, :128]
            for b in range(1, cols // 128):
                total += sq[:, :, b * 128 : (b + 1) * 128]
            lanes[pl.ds(p, m)] = total

    def finish(c, m, i):
        p = piece(c)
        some = pl.ds(c, m)

        @pl.when(c == free)
        def _():
            early(k).wait_recv()

        @pl.when(c >= free)
        def _():
            part[k, pl.ds(p, m)] += yrecv[k, pl.ds(jnp.maximum(c - free, 0), m)].astype(F32)

        for d in range(2):

            @pl.when(at[d] > 0)
            def _():
                along(d, n - 1, i, zsend.at[d, n - 2, some], zrecv.at[d, n - 2, some]).wait_recv()
                part[k, pl.ds(p, m)] += zrecv[d, n - 2, some].astype(F32)

        fsend[some] = part[k, pl.ds(p, m)].astype(BF16)
        final(c, m, i).start()

        @pl.when(c >= free)
        def _():
            put(p, m, fsend[some].astype(F32) * factor, lanes_s)

    def deliver(c, m, i):
        final(c, m, i).wait_recv()
        some = pl.ds(c, m)

        @pl.when(c < free)
        def _():
            put(piece(c), m, (fsend[some].astype(F32) + frecv[some].astype(F32)) * factor, lanes_u)

        @pl.when(c >= free)
        def _():
            put(mate * SPLIT + c - free, m, frecv[some].astype(F32) * factor, None)

    def energy(lanes):
        return jnp.sum(lanes[...].reshape(hidden_units, 128).T, axis=0, keepdims=True)

    def free_energy(to, slot):
        return pltpu.make_async_remote_copy(
            src_ref=esu, dst_ref=eru.at[slot], send_sem=us_sem.at[0], recv_sem=ur_sem.at[0],
            device_id={"fs": to}, device_id_type=MESH,
        )

    def split_energy(other, to, slot):
        return pltpu.make_async_remote_copy(
            src_ref=ess, dst_ref=ers.at[rep, slot], send_sem=ss_sem.at[other], recv_sem=sr_sem.at[other],
            device_id={"rep": jnp.where(other == 1, mate, rep), "fs": to}, device_id_type=MESH,
        )

    blocks = 4
    brows = tokens // blocks
    units = (n - 2) * halves

    def activations(i):
        at_rows = pl.ds(pl.multiple_of(i * brows, brows), brows)
        gate = g[at_rows, :].astype(F32)
        up = u[at_rows, :].astype(F32)
        grad = dhid[at_rows, :]
        sig = jax.nn.sigmoid(gate)
        du[at_rows, :] = (grad * (gate * sig)).astype(BF16)
        dg[at_rows, :] = (grad * up * sig * (1.0 + gate * (1.0 - sig))).astype(BF16)

    def last(c, m, i):
        finish(c, m, i)

        @pl.when(i < units)
        def _():
            gather(2 + i // halves, lax.rem(i, halves))

        @pl.when((i >= units) & (i < units + blocks))
        def _():
            activations(i - units)

        @pl.when(i >= LAG)
        def _():
            deliver(c - 2 * LAG, 2, i - LAG)

        @pl.when(i == free // 2 - 1 + LAG)
        def _():
            esu[...] = energy(lanes_u)
            for t in range(1, n):
                free_energy(lax.rem(k + t, n), k).start()

    steps(0, pairs, last)
    steps(pairs, end, finish)
    ess[...] = energy(lanes_s)
    for t in range(1, n):
        split_energy(0, lax.rem(k + t, n), k).start()
    for t in range(n):
        split_energy(1, lax.rem(k + t, n), k).start()
    steps(pairs - LAG, end, deliver)

    for d in range(2):

        @pl.when(at[d] < n - 1)
        def _():
            for s in range(n):
                whole = pltpu.make_async_remote_copy(
                    src_ref=zsend.at[d, 0], dst_ref=zrecv.at[d, 0], send_sem=zs_sem.at[d, s],
                    recv_sem=zr_sem.at[d, s, 0], device_id={"fs": k + sign[d]}, device_id_type=MESH,
                )
                whole.wait_send()

    across(fsend, frecv, fs_sem.at[0], fr_sem.at[0]).wait_send()
    across(ysend, yrecv, ys_sem.at[0], yr_sem.at[0]).wait_send()

    def sent_across(j):
        @pl.when(j != k)
        def _():
            crossing(j, rep, 0, SPLIT).wait_send()

    loop(0, n, sent_across)

    def settle(some, send, recv):
        copy = across(some, some, send, recv)
        copy.wait_send()
        copy.wait_recv()

    settle(eru.at[pl.ds(0, n - 1)], us_sem.at[0], ur_sem.at[0])
    settle(ers.at[0, pl.ds(0, n - 1)], ss_sem.at[0], sr_sem.at[0])
    settle(ers.at[1], ss_sem.at[1], sr_sem.at[1])
    total = jnp.zeros((1, hidden_units), F32)
    for j in range(n):
        total += jnp.where(j == k, esu[...], eru[j])
        for r in range(2):
            total += jnp.where((j == k) & (r == rep), ess[...], ers[r, j])
    en_ref[...] = total * (1.0 / width)


def write_out(dg, du, gd, en, dg_hbm, du_hbm, gd_hbm, en_out, sem):
    copies = [
        pltpu.make_async_copy(src, dst, sem.at[i])
        for i, (src, dst) in enumerate(((dg, dg_hbm), (du, du_hbm), (gd, gd_hbm)))
    ]
    for copy in copies:
        copy.start()
    en_out[...] = en[0, :]
    for copy in copies:
        copy.wait()


def fused(n, gate_pre, up_pre, out_grad, w_down):
    tokens, units = gate_pre.shape
    width = out_grad.shape[1]
    cols = w_down.shape[1]
    rows = units // PIECES
    count = PIECES - SPLIT
    factor = float(tokens * lax.axis_size("rep") * n) ** (-0.5)
    any_spec = pl.BlockSpec(memory_space=pl.ANY)
    vmem_spec = pl.BlockSpec(memory_space=pltpu.VMEM)
    dma = pltpu.SemaphoreType.DMA
    d_gate, d_up, grad, energy = pl.pallas_call(
        functools.partial(kernel, n, factor, width),
        out_shape=(
            pltpu.VMEM((tokens, units), BF16),
            pltpu.VMEM((tokens, units), BF16),
            pltpu.VMEM((PIECES, rows, cols), F32),
            pltpu.VMEM((1, units), F32),
        ),
        in_specs=[any_spec] * 4,
        out_specs=(vmem_spec,) * 4,
        scratch_shapes=[
            pltpu.VMEM((tokens, units), BF16),
            pltpu.VMEM((tokens, units), BF16),
            pltpu.VMEM((n, tokens, cols), BF16),
            pltpu.VMEM((n, PIECES, rows, cols), BF16),
            pltpu.VMEM((units, tokens), BF16),
            pltpu.VMEM((n, PIECES, rows, cols), F32),
            pltpu.VMEM((tokens, units), F32),
            pltpu.VMEM((2, n - 1, count, rows, cols), BF16),
            pltpu.VMEM((2, n - 1, count, rows, cols), BF16),
            pltpu.VMEM((n, SPLIT, rows, cols), BF16),
            pltpu.VMEM((n, SPLIT, rows, cols), BF16),
            pltpu.VMEM((count, rows, cols), BF16),
            pltpu.VMEM((count, rows, cols), BF16),
            pltpu.VMEM((PIECES, rows, 128), F32),
            pltpu.VMEM((PIECES, rows, 128), F32),
            pltpu.VMEM((1, units), F32),
            pltpu.VMEM((n, 1, units), F32),
            pltpu.VMEM((1, units), F32),
            pltpu.VMEM((2, n, 1, units), F32),
            dma((1 + 2 * LOADS,)),
            dma((n,)),
            dma((2, n)),
            dma((2, n, (count + 1) // 2)),
            dma((n,)),
            dma((n,)),
            dma((1,)),
            dma((n,)),
            dma((1,)),
            dma(((count + 1) // 2,)),
            dma((1,)),
            dma((1,)),
            dma((2,)),
            dma((2,)),
        ],
        compiler_params=pltpu.CompilerParams(
            collective_id=0, has_side_effects=True, vmem_limit_bytes=VMEM_LIMIT
        ),
    )(gate_pre, up_pre, out_grad, w_down.reshape(PIECES, rows, cols))
    return pl.pallas_call(
        write_out,
        out_shape=(
            jax.ShapeDtypeStruct((tokens, units), BF16),
            jax.ShapeDtypeStruct((tokens, units), BF16),
            jax.ShapeDtypeStruct((units, cols), F32),
            jax.ShapeDtypeStruct((units,), F32),
        ),
        in_specs=[vmem_spec] * 4,
        out_specs=(any_spec, any_spec, any_spec, vmem_spec),
        scratch_shapes=[dma((3,))],
        compiler_params=pltpu.CompilerParams(vmem_limit_bytes=4 * 1024 * 1024),
    )(d_gate, d_up, grad.reshape(units, cols), energy)


def solution(mesh):
    reps, n = mesh.shape["rep"], mesh.shape["fs"]

    def local(gate_pre, up_pre, out_grad, w_down):
        units, cols = w_down.shape
        fits = reps == 2 and 2 <= n <= 4 and cols % 128 == 0 and units % (PIECES * 16) == 0 and units % 128 == 0
        if fits and gate_pre.shape[0] % 1024 == 0:
            return fused(n, gate_pre, up_pre, out_grad, w_down)
        return plain(gate_pre, up_pre, out_grad, w_down)

    placed = (P(("rep", "fs"), "tp"), P(("rep", "fs"), "tp"), P(("rep", "fs"), None), P("tp", "fs"))
    return jax.shard_map(
        local,
        mesh=mesh,
        in_specs=placed,
        out_specs=(P(("rep", "fs"), "tp"), P(("rep", "fs"), "tp"), P("tp", "fs"), P("tp")),
        check_vma=False,
    )
```

time: 68.8 us -> 64 us (0.930)
  Pallas kernels: 68 us -> 63.2 us
    pallas_call x1, Pallas kernels: 65.3 us -> 60.5 us  [fused(): pl.pallas_call(functools.partial(kernel, n, factor, width), out_shape=(pl...]
where the time goes in v1:
time: 64 us; the launch traced here: 63.9 us
  Pallas kernels  63.2 us (99%)
  between operations  0.64 us (1%)
    pallas_call x1, Pallas kernels, fused(): pl.pallas_call(functools.partial(kernel, n, factor, width), out_shape=(pl...  60.5 us
    pallas_call x1, Pallas kernels, fused(): pl.pallas_call(write_out, out_shape=(jax.ShapeDtypeStruct((tokens, units)...  2.78 us

profile of v1, /device:TPU:0, one launch (start us, length us, event | category | flops | bytes accessed | tf_op | source)
XLA Modules:
  0.0 63.9 jit_solution(1554431675880755643)
XLA Ops:
  0.6 60.5 %shard_map.75 = (bf16[1024,768]{1,0:T(8,128)(2,1)S(1)}, bf16[1024,768]{1,0:T(8,128)(2,1)S(1)}, f32[24,32,512]{2,1,0:T(8,128)S(1)}, f32[1,768]{1,0:T(1,128)S(1)}) custom-call(bf16[1024,768]{1,0:T(8,128)(2,1)} %g_hbm.1, bf16[1024,768]{1,0:T(8,128)(2,1)} %u_hbm.1, bf16[1024,2048]{1,0:T(8,128)(2,1)} %og_hbm.1, bf16[24,32,512]{2,1,0:T(8,128)(2,1)} %bitcast.3), custom_call_target="tpu_custom_call" | custom-call | tf_op jit(solution)/shard_map/pallas_call | solution.py:424
  61.1 2.8 %shard_map.76 = (bf16[1024,768]{1,0:T(8,128)(2,1)}, bf16[1024,768]{1,0:T(8,128)(2,1)}, f32[768,512]{1,0:T(8,128)}, f32[768]{0:T(1024)}) custom-call(bf16[1024,768]{1,0:T(8,128)(2,1)S(1)} %get-tuple-element.8.dg, bf16[1024,768]{1,0:T(8,128)(2,1)S(1)} %get-tuple-element.9.du, f32[768,512]{1,0:T(8,128)S(1)} %bitcast.2, f32[1,768]{1,0:T(1,128)S(1)} %get-tuple-element.11.en), custom_call_target="tpu_custom_call" | custom-call | tf_op jit(solution)/shard_map/pallas_call | solution.py:473

commit v2 on v1

--- a/solution.py
+++ b/solution.py
@@ -10,11 +10,13 @@
 MESH = pl.DeviceIdType.MESH
 F32 = jnp.float32
 BF16 = jnp.bfloat16
-PIECES = 24
-SPLIT = 7
+PIECES = 16
+SPLIT = 5
+GROUP = 2
 LAG = 2
+NEAR = 2
 LOADS = 4
-BEFORE = 2
+BEFORE = 1
 VMEM_LIMIT = 52 * 1024 * 1024
 
 
@@ -60,7 +62,7 @@
     tokens = g.shape[0]
     count = PIECES - SPLIT
     free = PIECES - 2 * SPLIT
-    pairs = count // 2
+    pairs = count // GROUP
     chunk = tokens // LOADS
 
     def piece(c):
@@ -70,11 +72,11 @@
         lax.fori_loop(lo, hi, lambda i, x: (body(i), x)[1], 0)
 
     def steps(lo, hi, body):
-        loop(lo, min(hi, pairs), lambda i: body(2 * i, 2, i))
+        loop(lo, min(hi, pairs), lambda i: body(GROUP * i, GROUP, i))
         if hi > pairs:
-            body(k * 0 + 2 * pairs, 1, k * 0 + pairs)
-
-    end = pairs + count % 2
+            body(k * 0 + GROUP * pairs, count % GROUP, k * 0 + pairs)
+
+    end = -(-count // GROUP)
     low = jnp.minimum(k, n - 1 - k)
 
     def chosen(i):
@@ -84,11 +86,16 @@
     def rows_at(i):
         return pl.ds(pl.multiple_of(i * chunk, chunk), chunk)
 
-    def in_g(i):
-        return pltpu.make_async_copy(g_hbm.at[rows_at(i)], g.at[rows_at(i)], in_sem.at[1 + i])
-
-    def in_u(i):
-        return pltpu.make_async_copy(u_hbm.at[rows_at(i)], u.at[rows_at(i)], in_sem.at[1 + LOADS + i])
+    wide = -(-2 * SPLIT * rows // 128) * 128
+    spans = ((0, wide), (wide, hidden_units - wide)) if wide < hidden_units else ((0, wide),)
+
+    def in_gate(h, i):
+        at = (rows_at(i), pl.ds(*spans[h]))
+        return pltpu.make_async_copy(g_hbm.at[at], g.at[at], in_sem.at[1 + 2 * LOADS * h + i])
+
+    def in_up(h, i):
+        at = (rows_at(i), pl.ds(*spans[h]))
+        return pltpu.make_async_copy(u_hbm.at[at], u.at[at], in_sem.at[1 + 2 * LOADS * h + LOADS + i])
 
     def in_og(j):
         part_of = pl.ds(pl.multiple_of(j * cols, cols), cols)
@@ -108,17 +115,18 @@
     in_w = pltpu.make_async_copy(w_hbm, w.at[k], in_sem.at[0])
     in_w.start()
 
-    def load(i):
-        in_g(i).start()
-        in_u(i).start()
-
-    loop(0, LOADS, load)
-    loop(0, n, lambda i: in_og(chosen(i)).start())
-    lanes_u[...] = jnp.zeros_like(lanes_u)
-    lanes_s[...] = jnp.zeros_like(lanes_s)
+    def load(h, i):
+        in_gate(h, i).start()
+        in_up(h, i).start()
+
+    loop(0, LOADS, functools.partial(load, 0))
+    in_og(chosen(0)).start()
+    for h in range(1, len(spans)):
+        loop(0, LOADS, functools.partial(load, h))
+    loop(1, n, lambda i: in_og(chosen(i)).start())
     def along(d, s, i, src, dst):
         return pltpu.make_async_remote_copy(
-            src_ref=src, dst_ref=dst, send_sem=zs_sem.at[d, s], recv_sem=zr_sem.at[d, s, i],
+            src_ref=src, dst_ref=dst, send_sem=zs_sem.at[d], recv_sem=zr_sem.at[d, s % 3, i],
             device_id={"fs": k + sign[d]}, device_id_type=MESH,
         )
 
@@ -136,17 +144,18 @@
 
     def crossing(j, owner, start, m):
         block = w.at[j, pl.ds(owner * SPLIT + start, m)]
-        return across(block, block, as_sem.at[j], ar_sem.at[j])
-
-    def make_hidden(i):
-        in_g(i).wait()
-        in_u(i).wait()
-        gate = g[rows_at(i), :].astype(F32)
+        return across(block, block, as_sem.at[0], ar_sem.at[j])
+
+    def make_hidden(h, i):
+        in_gate(h, i).wait()
+        in_up(h, i).wait()
+        start, width = spans[h]
+        at = (rows_at(i), pl.ds(start, width))
+        gate = g[at].astype(F32)
         act = gate * jax.nn.sigmoid(gate)
-        h = (act * u[rows_at(i), :].astype(F32)).astype(BF16)
-        hid[:, rows_at(i)] = h.T
-
-    loop(0, BEFORE, make_hidden)
+        hid[pl.ds(start, width), rows_at(i)] = (act * u[at].astype(F32)).astype(BF16).T
+
+    loop(0, BEFORE, functools.partial(make_hidden, 0))
     pl.semaphore_wait(barrier, 1 + (k > 0).astype(jnp.int32) + (k < n - 1).astype(jnp.int32))
     in_w.wait()
 
@@ -159,21 +168,28 @@
                 along(d, 0, i, block, block).start()
 
     steps(0, end, first)
-    loop(BEFORE, LOADS, make_hidden)
+    loop(BEFORE, LOADS, functools.partial(make_hidden, 0))
 
     def product(j, start, pieces):
         some = hid[pl.ds(pl.multiple_of(start * rows, rows), pieces * rows), :]
         return jnp.dot(some, og[j], preferred_element_type=F32).reshape(pieces, rows, cols)
 
-    def make_part(i):
+    def make_early(i):
         j = chosen(i)
         in_og(j).wait()
         ysend[j] = product(j, mate * SPLIT, SPLIT).astype(BF16)
         early(j).start()
+
+    def make_part(j):
         part[j, pl.ds(2 * SPLIT, free)] = product(j, 2 * SPLIT, free)
         part[j, pl.ds(rep * SPLIT, SPLIT)] = product(j, rep * SPLIT, SPLIT)
 
+    loop(0, n, make_early)
+    for h in range(1, len(spans)):
+        loop(0, LOADS, functools.partial(make_hidden, h))
     loop(0, n, make_part)
+    lanes_u[...] = jnp.zeros_like(lanes_u)
+    lanes_s[...] = jnp.zeros_like(lanes_s)
 
     def multiply(j, at_rows):
         return lax.dot_general(
@@ -253,9 +269,9 @@
 
     for s in range(1, n - 1):
         steps(0, end, functools.partial(pass_on, s))
-    steps(0, pairs - 2, functools.partial(pass_on, n - 1))
+    steps(0, NEAR, functools.partial(pass_on, n - 1))
     loop(0, halves, functools.partial(gather, 1))
-    steps(pairs - 2, end, functools.partial(pass_on, n - 1))
+    steps(NEAR, end, functools.partial(pass_on, n - 1))
 
     def put(p, m, value, lanes):
         gd[pl.ds(p, m)] = value
@@ -322,6 +338,7 @@
     blocks = 4
     brows = tokens // blocks
     units = (n - 2) * halves
+    each = -(-(units + blocks) // (end - 1))
 
     def activations(i):
         at_rows = pl.ds(pl.multiple_of(i * brows, brows), brows)
@@ -335,53 +352,47 @@
     def last(c, m, i):
         finish(c, m, i)
 
-        @pl.when(i < units)
-        def _():
-            gather(2 + i // halves, lax.rem(i, halves))
-
-        @pl.when((i >= units) & (i < units + blocks))
-        def _():
-            activations(i - units)
+        for a in range(each):
+            q = i * each + a
+
+            @pl.when(q < units)
+            def _():
+                gather(2 + q // halves, lax.rem(q, halves))
+
+            @pl.when((q >= units) & (q < units + blocks))
+            def _():
+                activations(q - units)
 
         @pl.when(i >= LAG)
         def _():
-            deliver(c - 2 * LAG, 2, i - LAG)
-
-        @pl.when(i == free // 2 - 1 + LAG)
+            deliver(c - GROUP * LAG, GROUP, i - LAG)
+
+        @pl.when(i == free // GROUP - 1 + LAG)
         def _():
             esu[...] = energy(lanes_u)
             for t in range(1, n):
                 free_energy(lax.rem(k + t, n), k).start()
 
-    steps(0, pairs, last)
-    steps(pairs, end, finish)
+    steps(0, end - 1, last)
+    steps(end - 1, end, finish)
     ess[...] = energy(lanes_s)
     for t in range(1, n):
         split_energy(0, lax.rem(k + t, n), k).start()
     for t in range(n):
         split_energy(1, lax.rem(k + t, n), k).start()
-    steps(pairs - LAG, end, deliver)
+    steps(end - 1 - LAG, end, deliver)
 
     for d in range(2):
 
         @pl.when(at[d] < n - 1)
         def _():
-            for s in range(n):
-                whole = pltpu.make_async_remote_copy(
-                    src_ref=zsend.at[d, 0], dst_ref=zrecv.at[d, 0], send_sem=zs_sem.at[d, s],
-                    recv_sem=zr_sem.at[d, s, 0], device_id={"fs": k + sign[d]}, device_id_type=MESH,
-                )
-                whole.wait_send()
+            along(d, 0, 0, w.at[:, pl.ds(0, count)], w.at[:, pl.ds(0, count)]).wait_send()
 
     across(fsend, frecv, fs_sem.at[0], fr_sem.at[0]).wait_send()
     across(ysend, yrecv, ys_sem.at[0], yr_sem.at[0]).wait_send()
 
-    def sent_across(j):
-        @pl.when(j != k)
-        def _():
-            crossing(j, rep, 0, SPLIT).wait_send()
-
-    loop(0, n, sent_across)
+    crossed = w.at[pl.ds(0, n - 1), pl.ds(0, SPLIT)]
+    across(crossed, crossed, as_sem.at[0], ar_sem.at[0]).wait_send()
 
     def settle(some, send, recv):
         copy = across(some, some, send, recv)
@@ -399,14 +410,16 @@
     en_ref[...] = total * (1.0 / width)
 
 
-def write_out(dg, du, gd, en, dg_hbm, du_hbm, gd_hbm, en_out, sem):
-    copies = [
-        pltpu.make_async_copy(src, dst, sem.at[i])
-        for i, (src, dst) in enumerate(((dg, dg_hbm), (du, du_hbm), (gd, gd_hbm)))
-    ]
+def write_out(dg, du, gd, en, dg_hbm, du_hbm, gd_hbm, en_hbm, flat, sem):
+    def copy_of(i, src, dst):
+        return pltpu.make_async_copy(src, dst, sem.at[i])
+
+    copies = [copy_of(0, dg, dg_hbm), copy_of(1, du, du_hbm), copy_of(2, gd, gd_hbm)]
     for copy in copies:
         copy.start()
-    en_out[...] = en[0, :]
+    flat[...] = en[0, :]
+    copies.append(copy_of(3, flat, en_hbm))
+    copies[3].start()
     for copy in copies:
         copy.wait()
 
@@ -451,16 +464,16 @@
             pltpu.VMEM((n, 1, units), F32),
             pltpu.VMEM((1, units), F32),
             pltpu.VMEM((2, n, 1, units), F32),
-            dma((1 + 2 * LOADS,)),
+            dma((1 + 4 * LOADS,)),
             dma((n,)),
-            dma((2, n)),
-            dma((2, n, (count + 1) // 2)),
-            dma((n,)),
+            dma((2,)),
+            dma((2, min(n, 3), -(-count // GROUP))),
+            dma((1,)),
             dma((n,)),
             dma((1,)),
             dma((n,)),
             dma((1,)),
-            dma(((count + 1) // 2,)),
+            dma((-(-count // GROUP),)),
             dma((1,)),
             dma((1,)),
             dma((2,)),
@@ -479,8 +492,8 @@
             jax.ShapeDtypeStruct((units,), F32),
         ),
         in_specs=[vmem_spec] * 4,
-        out_specs=(any_spec, any_spec, any_spec, vmem_spec),
-        scratch_shapes=[dma((3,))],
+        out_specs=(any_spec,) * 4,
+        scratch_shapes=[pltpu.VMEM((units,), F32), dma((4,))],
         compiler_params=pltpu.CompilerParams(vmem_limit_bytes=4 * 1024 * 1024),
     )(d_gate, d_up, grad.reshape(units, cols), energy)
 

time: 64 us -> 60.8 us (0.950)
  Pallas kernels: 63.2 us -> 60 us
    pallas_call x1, Pallas kernels: 60.5 us -> 57.8 us  [fused(): pl.pallas_call(functools.partial(kernel, n, factor, width), out_shape=(pl...]
where the time goes in v2:
time: 60.8 us; the launch traced here: 60.7 us
  Pallas kernels  60 us (99%)
  between operations  0.64 us (1%)
    pallas_call x1, Pallas kernels, fused(): pl.pallas_call(functools.partial(kernel, n, factor, width), out_shape=(pl...  57.8 us
    pallas_call x1, Pallas kernels, fused(): pl.pallas_call(write_out, out_shape=(jax.ShapeDtypeStruct((tokens, units)...  2.22 us

profile of v2, /device:TPU:0, one launch (start us, length us, event | category | flops | bytes accessed | tf_op | source)
XLA Modules:
  0.0 60.7 jit_solution(8403106455091638840)
XLA Ops:
  0.6 57.8 %shard_map.75 = (bf16[1024,768]{1,0:T(8,128)(2,1)S(1)}, bf16[1024,768]{1,0:T(8,128)(2,1)S(1)}, f32[16,48,512]{2,1,0:T(8,128)S(1)}, f32[1,768]{1,0:T(1,128)S(1)}) custom-call(bf16[1024,768]{1,0:T(8,128)(2,1)} %g_hbm.1, bf16[1024,768]{1,0:T(8,128)(2,1)} %u_hbm.1, bf16[1024,2048]{1,0:T(8,128)(2,1)} %og_hbm.1, bf16[16,48,512]{2,1,0:T(8,128)(2,1)} %bitcast.3), custom_call_target="tpu_custom_call" | custom-call | tf_op jit(solution)/shard_map/pallas_call | solution.py:437
  58.5 2.2 %shard_map.76 = (bf16[1024,768]{1,0:T(8,128)(2,1)}, bf16[1024,768]{1,0:T(8,128)(2,1)}, f32[768,512]{1,0:T(8,128)}, f32[768]{0:T(1024)}) custom-call(bf16[1024,768]{1,0:T(8,128)(2,1)S(1)} %get-tuple-element.8.dg, bf16[1024,768]{1,0:T(8,128)(2,1)S(1)} %get-tuple-element.9.du, f32[768,512]{1,0:T(8,128)S(1)} %bitcast.2, f32[1,768]{1,0:T(1,128)S(1)} %get-tuple-element.11.en), custom_call_target="tpu_custom_call" | custom-call | tf_op jit(solution)/shard_map/pallas_call | solution.py:486

commit v3 on v2

--- a/solution.py
+++ b/solution.py
@@ -13,10 +13,10 @@
 PIECES = 16
 SPLIT = 5
 GROUP = 2
-LAG = 2
-NEAR = 2
+FIRST = 2
+FROM = 1
 LOADS = 4
-BEFORE = 1
+BEFORE = 0
 VMEM_LIMIT = 52 * 1024 * 1024
 
 
@@ -50,7 +50,7 @@
     dg, du, gd, en_ref,
     g, u, og, w, hid, part, dhid, zsend, zrecv, ysend, yrecv, fsend, frecv,
     lanes_u, lanes_s, esu, eru, ess, ers,
-    in_sem, og_sem, zs_sem, zr_sem, as_sem, ar_sem, ys_sem, yr_sem, fs_sem, fr_sem,
+    in_sem, og_sem, zs_sem, zr_sem, zx_sem, as_sem, ar_sem, ys_sem, yr_sem, fs_sem, fr_sem,
     us_sem, ur_sem, ss_sem, sr_sem,
 ):
     rep = lax.axis_index("rep")
@@ -77,6 +77,7 @@
             body(k * 0 + GROUP * pairs, count % GROUP, k * 0 + pairs)
 
     end = -(-count // GROUP)
+    late = free // GROUP - 1
     low = jnp.minimum(k, n - 1 - k)
 
     def chosen(i):
@@ -90,12 +91,12 @@
     spans = ((0, wide), (wide, hidden_units - wide)) if wide < hidden_units else ((0, wide),)
 
     def in_gate(h, i):
-        at = (rows_at(i), pl.ds(*spans[h]))
-        return pltpu.make_async_copy(g_hbm.at[at], g.at[at], in_sem.at[1 + 2 * LOADS * h + i])
+        at = (rows_at(i) if h == 0 else pl.ds(0, tokens), pl.ds(*spans[h]))
+        return pltpu.make_async_copy(g_hbm.at[at], g.at[at], in_sem.at[4 + 2 * i if h == 0 else 2])
 
     def in_up(h, i):
-        at = (rows_at(i), pl.ds(*spans[h]))
-        return pltpu.make_async_copy(u_hbm.at[at], u.at[at], in_sem.at[1 + 2 * LOADS * h + LOADS + i])
+        at = (rows_at(i) if h == 0 else pl.ds(0, tokens), pl.ds(*spans[h]))
+        return pltpu.make_async_copy(u_hbm.at[at], u.at[at], in_sem.at[5 + 2 * i if h == 0 else 3])
 
     def in_og(j):
         part_of = pl.ds(pl.multiple_of(j * cols, cols), cols)
@@ -112,8 +113,12 @@
             pl.semaphore_signal(barrier, inc=1, device_id={"fs": k + sign[d]}, device_id_type=MESH)
 
     pl.semaphore_signal(barrier, inc=1, device_id={"rep": mate}, device_id_type=MESH)
-    in_w = pltpu.make_async_copy(w_hbm, w.at[k], in_sem.at[0])
-    in_w.start()
+    in_w = [
+        pltpu.make_async_copy(w_hbm.at[some], w.at[k, some], in_sem.at[i])
+        for i, some in enumerate((pl.ds(2 * SPLIT, free), pl.ds(0, 2 * SPLIT)))
+    ]
+    for copy in in_w:
+        copy.start()
 
     def load(h, i):
         in_gate(h, i).start()
@@ -122,11 +127,50 @@
     loop(0, LOADS, functools.partial(load, 0))
     in_og(chosen(0)).start()
     for h in range(1, len(spans)):
-        loop(0, LOADS, functools.partial(load, h))
+        load(h, 0)
     loop(1, n, lambda i: in_og(chosen(i)).start())
-    def along(d, s, i, src, dst):
+    def along(d, s, i, src, dst, kind=0):
         return pltpu.make_async_remote_copy(
-            src_ref=src, dst_ref=dst, send_sem=zs_sem.at[d], recv_sem=zr_sem.at[d, s % 3, i],
+            src_ref=src, dst_ref=dst, send_sem=zs_sem.at[d, kind], recv_sem=zr_sem.at[d, lax.rem(s * end + i, 2 * end + 1)],
+            device_id={"fs": k + sign[d]}, device_id_type=MESH,
+        )
+
+    def block_of(j, p, m, i):
+        brief = (i == 0) & (rep == 1) & (j == n - 1)
+
+        def each_size(act):
+            @pl.when(brief)
+            def _():
+                act(w.at[j, pl.ds(p, m - 1)])
+
+            @pl.when(jnp.logical_not(brief))
+            def _():
+                act(w.at[j, pl.ds(p, m)])
+
+        return each_size
+
+    def spread(pieces):
+        blocks = next(b for b in range(1, n + 1) if pieces % b == 0 and pieces // b <= PIECES)
+        return w.at[pl.ds(0, blocks), pl.ds(0, pieces // blocks)]
+
+    def send_block(d, s, i, j, p, m):
+        if m > 1:
+            block_of(j, p, m, i)(lambda block: along(d, s, i, block, block).start())
+        else:
+            block = w.at[j, pl.ds(p, m)]
+            along(d, s, i, block, block).start()
+
+    def take_block(d, s, i, j, p, m):
+        if m > 1:
+            block_of(j, p, m, i)(lambda block: along(d, s, i, block, block).wait_recv())
+        else:
+            block = w.at[j, pl.ds(p, m)]
+            along(d, s, i, block, block).wait_recv()
+
+    def deferred(d):
+        block = w.at[k, pl.ds(2 * SPLIT + late * GROUP, GROUP)]
+        return pltpu.make_async_remote_copy(
+            src_ref=block, dst_ref=block, send_sem=zs_sem.at[d, 0], recv_sem=zx_sem.at[d],
             device_id={"fs": k + sign[d]}, device_id_type=MESH,
         )
 
@@ -146,9 +190,13 @@
         block = w.at[j, pl.ds(owner * SPLIT + start, m)]
         return across(block, block, as_sem.at[0], ar_sem.at[j])
 
-    def make_hidden(h, i):
+    def loaded(h, i):
         in_gate(h, i).wait()
         in_up(h, i).wait()
+
+    def make_hidden(h, i):
+        if h == 0:
+            loaded(h, i)
         start, width = spans[h]
         at = (rows_at(i), pl.ds(start, width))
         gate = g[at].astype(F32)
@@ -157,17 +205,18 @@
 
     loop(0, BEFORE, functools.partial(make_hidden, 0))
     pl.semaphore_wait(barrier, 1 + (k > 0).astype(jnp.int32) + (k < n - 1).astype(jnp.int32))
-    in_w.wait()
+    in_w[0].wait()
 
     def first(c, m, i):
         for d in range(2):
 
-            @pl.when(at[d] < n - 1)
-            def _():
-                block = w.at[k, pl.ds(piece(c), m)]
-                along(d, 0, i, block, block).start()
-
-    steps(0, end, first)
+            @pl.when((at[d] < n - 2) | ((at[d] == n - 2) & (i != late)))
+            def _():
+                send_block(d, 0, i, k, piece(c), m)
+
+    steps(0, free // GROUP, first)
+    in_w[1].wait()
+    steps(free // GROUP, end, first)
     loop(BEFORE, LOADS, functools.partial(make_hidden, 0))
 
     def product(j, start, pieces):
@@ -186,6 +235,7 @@
 
     loop(0, n, make_early)
     for h in range(1, len(spans)):
+        loaded(h, 0)
         loop(0, LOADS, functools.partial(make_hidden, h))
     loop(0, n, make_part)
     lanes_u[...] = jnp.zeros_like(lanes_u)
@@ -209,22 +259,34 @@
             place = at[d]
             some = pl.ds(c, m)
 
-            @pl.when(place > 0)
+            came = place > 0
+            if s == 1:
+                came &= (place < n - 1) | (i != late)
+
+            @pl.when(came & (s > place))
             def _():
                 along(d, s - 1, i, zsend.at[d, 0, some], zrecv.at[d, 0, some]).wait_recv()
 
             @pl.when(s <= place)
             def _():
                 j = k - sign[d] * s
-                block = w.at[j, pl.ds(p, m)]
+
+                @pl.when(came)
+                def _():
+                    take_block(d, s - 1, i, j, p, m)
 
                 @pl.when(place < n - 1)
                 def _():
-                    along(d, s, i, block, block).start()
+                    send_block(d, s, i, j, p, m)
 
                 @pl.when(c >= free)
                 def _():
                     crossing(j, rep, c - free, m).start()
+
+                @pl.when((i == 0) & (rep == 0) & (j == n - 1))
+                def _():
+                    extra = w.at[j, pl.ds(2 * SPLIT + GROUP - 1, 1)]
+                    across(extra, extra, as_sem.at[0], ar_sem.at[j]).start()
 
             @pl.when(s > place)
             def _():
@@ -245,33 +307,46 @@
                         part[j, pl.ds(p, m)] += zrecv[d, s - 2, some].astype(F32)
 
                 zsend[d, s - 1, some] = part[j, pl.ds(p, m)].astype(BF16)
-                along(d, s, i, zsend.at[d, s - 1, some], zrecv.at[d, s - 1, some]).start()
+                along(d, s, i, zsend.at[d, s - 1, some], zrecv.at[d, s - 1, some], 1).start()
 
     def gathered(j):
-        crossing(j, mate, 0, SPLIT).wait_recv()
+        for r in range(2):
+
+            @pl.when(((rep == 1) & (j == n - 1)) == (r == 1))
+            def _():
+                some = w.at[j, pl.ds(0, SPLIT + r)]
+                across(some, some, as_sem.at[0], ar_sem.at[j]).wait_recv()
 
     halves = 2
     half = tokens // halves
 
-    def gather(far, part_of):
+    def gather(far, part_of, ends=None):
         at_rows = pl.ds(pl.multiple_of(part_of * half, half), half)
         for d in range(2):
-
-            @pl.when(at[d] >= far)
+            here = at[d] >= far
+            if ends is not None:
+                here &= (at[d] == n - 1) == ends
+
+            @pl.when(here)
             def _():
                 j = k - sign[d] * far
 
                 @pl.when(part_of == 0)
                 def _():
                     gathered(j)
+                    if ends:
+                        deferred(d).wait_recv()
 
                 dhid[at_rows, :] += multiply(j, at_rows)
 
     for s in range(1, n - 1):
         steps(0, end, functools.partial(pass_on, s))
-    steps(0, NEAR, functools.partial(pass_on, n - 1))
-    loop(0, halves, functools.partial(gather, 1))
-    steps(NEAR, end, functools.partial(pass_on, n - 1))
+    steps(0, end, functools.partial(pass_on, n - 1))
+    for d in range(2):
+
+        @pl.when(at[d] == n - 2)
+        def _():
+            deferred(d).start()
 
     def put(p, m, value, lanes):
         gd[pl.ds(p, m)] = value
@@ -337,8 +412,6 @@
 
     blocks = 4
     brows = tokens // blocks
-    units = (n - 2) * halves
-    each = -(-(units + blocks) // (end - 1))
 
     def activations(i):
         at_rows = pl.ds(pl.multiple_of(i * brows, brows), brows)
@@ -352,26 +425,13 @@
     def last(c, m, i):
         finish(c, m, i)
 
-        for a in range(each):
-            q = i * each + a
-
-            @pl.when(q < units)
-            def _():
-                gather(2 + q // halves, lax.rem(q, halves))
-
-            @pl.when((q >= units) & (q < units + blocks))
-            def _():
-                activations(q - units)
-
-        @pl.when(i >= LAG)
-        def _():
-            deliver(c - GROUP * LAG, GROUP, i - LAG)
-
-        @pl.when(i == free // GROUP - 1 + LAG)
-        def _():
-            esu[...] = energy(lanes_u)
-            for t in range(1, n):
-                free_energy(lax.rem(k + t, n), k).start()
+        @pl.when((i >= FROM) & (i < FROM + halves))
+        def _():
+            gather(1, i - FROM, ends=False)
+
+        @pl.when((i >= FROM + halves) & (i < FROM + halves + n - 2))
+        def _():
+            loop(0, halves, functools.partial(gather, 2 + i - FROM - halves))
 
     steps(0, end - 1, last)
     steps(end - 1, end, finish)
@@ -380,19 +440,50 @@
         split_energy(0, lax.rem(k + t, n), k).start()
     for t in range(n):
         split_energy(1, lax.rem(k + t, n), k).start()
-    steps(end - 1 - LAG, end, deliver)
+
+    def outputs():
+        @pl.when((k == 0) | (k == n - 1))
+        def _():
+            loop(0, halves, functools.partial(gather, 1, ends=True))
+
+        loop(0, blocks, activations)
+
+    @pl.when(rep == FIRST)
+    def _():
+        outputs()
+
+    steps(0, free // GROUP, deliver)
+    esu[...] = energy(lanes_u)
+    for t in range(1, n):
+        free_energy(lax.rem(k + t, n), k).start()
+
+    @pl.when(rep != FIRST)
+    def _():
+        outputs()
+
+    steps(free // GROUP, end, deliver)
 
     for d in range(2):
 
-        @pl.when(at[d] < n - 1)
-        def _():
-            along(d, 0, 0, w.at[:, pl.ds(0, count)], w.at[:, pl.ds(0, count)]).wait_send()
+        for p in range(n - 1):
+            for r in range(2):
+
+                @pl.when((at[d] == p) & (rep == r))
+                def _():
+                    sent = spread((p + 1) * count - r * d)
+                    along(d, 0, 0, sent, sent).wait_send()
+                    sent = zsend.at[d, pl.ds(0, n - 1 - p)]
+                    along(d, 0, 0, sent, sent, 1).wait_send()
 
     across(fsend, frecv, fs_sem.at[0], fr_sem.at[0]).wait_send()
     across(ysend, yrecv, ys_sem.at[0], yr_sem.at[0]).wait_send()
 
-    crossed = w.at[pl.ds(0, n - 1), pl.ds(0, SPLIT)]
-    across(crossed, crossed, as_sem.at[0], ar_sem.at[0]).wait_send()
+    for r in range(2):
+
+        @pl.when(((rep == 0) & (k < n - 1)) == (r == 1))
+        def _():
+            crossed = spread((n - 1) * SPLIT + r)
+            across(crossed, crossed, as_sem.at[0], ar_sem.at[0]).wait_send()
 
     def settle(some, send, recv):
         copy = across(some, some, send, recv)
@@ -464,10 +555,11 @@
             pltpu.VMEM((n, 1, units), F32),
             pltpu.VMEM((1, units), F32),
             pltpu.VMEM((2, n, 1, units), F32),
-            dma((1 + 4 * LOADS,)),
+            dma((4 + 2 * LOADS,)),
             dma((n,)),
+            dma((2, 2)),
+            dma((2, 2 * -(-count // GROUP) + 1)),
             dma((2,)),
-            dma((2, min(n, 3), -(-count // GROUP))),
             dma((1,)),
             dma((n,)),
             dma((1,)),

time: 60.8 us -> 60 us (0.987)
  Pallas kernels: 60 us -> 59.2 us
    pallas_call x1, Pallas kernels: 57.8 us -> 57 us  [fused(): pl.pallas_call(functools.partial(kernel, n, factor, width), out_shape=(pl...]
where the time goes in v3:
time: 60 us; the launch traced here: 59.9 us
  Pallas kernels  59.2 us (99%)
  between operations  0.64 us (1%)
    pallas_call x1, Pallas kernels, fused(): pl.pallas_call(functools.partial(kernel, n, factor, width), out_shape=(pl...  57 us
    pallas_call x1, Pallas kernels, fused(): pl.pallas_call(write_out, out_shape=(jax.ShapeDtypeStruct((tokens, units)...  2.22 us

profile of v3, /device:TPU:0, one launch (start us, length us, event | category | flops | bytes accessed | tf_op | source)
XLA Modules:
  0.0 59.9 jit_solution(5105727631904351876)
XLA Ops:
  0.6 57.0 %shard_map.75 = (bf16[1024,768]{1,0:T(8,128)(2,1)S(1)}, bf16[1024,768]{1,0:T(8,128)(2,1)S(1)}, f32[16,48,512]{2,1,0:T(8,128)S(1)}, f32[1,768]{1,0:T(1,128)S(1)}) custom-call(bf16[1024,768]{1,0:T(8,128)(2,1)} %g_hbm.1, bf16[1024,768]{1,0:T(8,128)(2,1)} %u_hbm.1, bf16[1024,2048]{1,0:T(8,128)(2,1)} %og_hbm.1, bf16[16,48,512]{2,1,0:T(8,128)(2,1)} %bitcast.3), custom_call_target="tpu_custom_call" | custom-call | tf_op jit(solution)/shard_map/pallas_call | solution.py:528
  57.7 2.2 %shard_map.76 = (bf16[1024,768]{1,0:T(8,128)(2,1)}, bf16[1024,768]{1,0:T(8,128)(2,1)}, f32[768,512]{1,0:T(8,128)}, f32[768]{0:T(1024)}) custom-call(bf16[1024,768]{1,0:T(8,128)(2,1)S(1)} %get-tuple-element.8.dg, bf16[1024,768]{1,0:T(8,128)(2,1)S(1)} %get-tuple-element.9.du, f32[768,512]{1,0:T(8,128)S(1)} %bitcast.2, f32[1,768]{1,0:T(1,128)S(1)} %get-tuple-element.11.en), custom_call_target="tpu_custom_call" | custom-call | tf_op jit(solution)/shard_map/pallas_call | solution.py:578

commit v4 on v3

--- a/solution.py
+++ b/solution.py
@@ -92,11 +92,11 @@
 
     def in_gate(h, i):
         at = (rows_at(i) if h == 0 else pl.ds(0, tokens), pl.ds(*spans[h]))
-        return pltpu.make_async_copy(g_hbm.at[at], g.at[at], in_sem.at[4 + 2 * i if h == 0 else 2])
+        return pltpu.make_async_copy(g_hbm.at[at], g.at[at], in_sem.at[3 + i if h == 0 else 2])
 
     def in_up(h, i):
         at = (rows_at(i) if h == 0 else pl.ds(0, tokens), pl.ds(*spans[h]))
-        return pltpu.make_async_copy(u_hbm.at[at], u.at[at], in_sem.at[5 + 2 * i if h == 0 else 3])
+        return pltpu.make_async_copy(u_hbm.at[at], u.at[at], in_sem.at[3 + i if h == 0 else 2])
 
     def in_og(j):
         part_of = pl.ds(pl.multiple_of(j * cols, cols), cols)
@@ -184,15 +184,16 @@
         return across(ysend.at[j], yrecv.at[j], ys_sem.at[0], yr_sem.at[j])
 
     def final(c, m, i):
-        return across(fsend.at[pl.ds(c, m)], frecv.at[pl.ds(c, m)], fs_sem.at[0], fr_sem.at[i])
+        return across(fsend.at[pl.ds(c, m)], frecv.at[pl.ds(c, m)], fs_sem.at[0], fr_sem.at[(i >= free // GROUP).astype(jnp.int32)])
 
     def crossing(j, owner, start, m):
         block = w.at[j, pl.ds(owner * SPLIT + start, m)]
         return across(block, block, as_sem.at[0], ar_sem.at[j])
 
     def loaded(h, i):
-        in_gate(h, i).wait()
-        in_up(h, i).wait()
+        both = (pl.ds(0, 2 * chunk), pl.ds(*spans[0])) if h == 0 else (pl.ds(0, tokens), pl.ds(0, 2 * spans[h][1]))
+        sem = in_sem.at[3 + i if h == 0 else 2]
+        pltpu.make_async_copy(g_hbm.at[both], g.at[both], sem).wait()
 
     def make_hidden(h, i):
         if h == 0:
@@ -384,7 +385,6 @@
             put(p, m, fsend[some].astype(F32) * factor, lanes_s)
 
     def deliver(c, m, i):
-        final(c, m, i).wait_recv()
         some = pl.ds(c, m)
 
         @pl.when(c < free)
@@ -452,6 +452,11 @@
     def _():
         outputs()
 
+    def arrived(start, pieces, slot):
+        some = pl.ds(start, pieces)
+        across(fsend.at[some], frecv.at[some], fs_sem.at[0], fr_sem.at[slot]).wait_recv()
+
+    arrived(0, free, 0)
     steps(0, free // GROUP, deliver)
     esu[...] = energy(lanes_u)
     for t in range(1, n):
@@ -461,6 +466,7 @@
     def _():
         outputs()
 
+    arrived(free, SPLIT, 1)
     steps(free // GROUP, end, deliver)
 
     for d in range(2):
@@ -555,7 +561,7 @@
             pltpu.VMEM((n, 1, units), F32),
             pltpu.VMEM((1, units), F32),
             pltpu.VMEM((2, n, 1, units), F32),
-            dma((4 + 2 * LOADS,)),
+            dma((3 + LOADS,)),
             dma((n,)),
             dma((2, 2)),
             dma((2, 2 * -(-count // GROUP) + 1)),
@@ -565,7 +571,7 @@
             dma((1,)),
             dma((n,)),
             dma((1,)),
-            dma((-(-count // GROUP),)),
+            dma((2,)),
             dma((1,)),
             dma((1,)),
             dma((2,)),

time: 60 us -> 59.9 us (level)
  no operation moved by 1% of the time
where the time goes in v4:
time: 59.9 us; the launch traced here: 59.7 us
  Pallas kernels  59.1 us (99%)
  between operations  0.64 us (1%)
    pallas_call x1, Pallas kernels, fused(): pl.pallas_call(functools.partial(kernel, n, factor, width), out_shape=(pl...  56.9 us
    pallas_call x1, Pallas kernels, fused(): pl.pallas_call(write_out, out_shape=(jax.ShapeDtypeStruct((tokens, units)...  2.22 us

profile of v4, /device:TPU:0, one launch (start us, length us, event | category | flops | bytes accessed | tf_op | source)
XLA Modules:
  0.0 59.7 jit_solution(5574828991748640608)
XLA Ops:
  0.6 56.9 %shard_map.75 = (bf16[1024,768]{1,0:T(8,128)(2,1)S(1)}, bf16[1024,768]{1,0:T(8,128)(2,1)S(1)}, f32[16,48,512]{2,1,0:T(8,128)S(1)}, f32[1,768]{1,0:T(1,128)S(1)}) custom-call(bf16[1024,768]{1,0:T(8,128)(2,1)} %g_hbm.1, bf16[1024,768]{1,0:T(8,128)(2,1)} %u_hbm.1, bf16[1024,2048]{1,0:T(8,128)(2,1)} %og_hbm.1, bf16[16,48,512]{2,1,0:T(8,128)(2,1)} %bitcast.3), custom_call_target="tpu_custom_call" | custom-call | tf_op jit(solution)/shard_map/pallas_call | solution.py:534
  57.5 2.2 %shard_map.76 = (bf16[1024,768]{1,0:T(8,128)(2,1)}, bf16[1024,768]{1,0:T(8,128)(2,1)}, f32[768,512]{1,0:T(8,128)}, f32[768]{0:T(1024)}) custom-call(bf16[1024,768]{1,0:T(8,128)(2,1)S(1)} %get-tuple-element.8.dg, bf16[1024,768]{1,0:T(8,128)(2,1)S(1)} %get-tuple-element.9.du, f32[768,512]{1,0:T(8,128)S(1)} %bitcast.2, f32[1,768]{1,0:T(1,128)S(1)} %get-tuple-element.11.en), custom_call_target="tpu_custom_call" | custom-call | tf_op jit(solution)/shard_map/pallas_call | solution.py:584

commit v5 on v4

--- a/solution.py
+++ b/solution.py
@@ -240,6 +240,7 @@
         loop(0, LOADS, functools.partial(make_hidden, h))
     loop(0, n, make_part)
     lanes_u[...] = jnp.zeros_like(lanes_u)
+    esu[...] = jnp.zeros_like(esu)
     lanes_s[...] = jnp.zeros_like(lanes_s)
 
     def multiply(j, at_rows):
@@ -458,7 +459,10 @@
 
     arrived(0, free, 0)
     steps(0, free // GROUP, deliver)
-    esu[...] = energy(lanes_u)
+    base = 2 * SPLIT * rows // 128 * 128
+    base = base if base % rows == 0 else 0
+    tail = lanes_u[base // rows :].reshape(hidden_units - base, 128)
+    esu[:, base:] = jnp.sum(tail.T, axis=0, keepdims=True)
     for t in range(1, n):
         free_energy(lax.rem(k + t, n), k).start()
 

time: 59.9 us -> 59.9 us (level)
  no operation moved by 1% of the time
where the time goes in v5:
time: 59.9 us; the launch traced here: 59.7 us
  Pallas kernels  59.1 us (99%)
  between operations  0.64 us (1%)
    pallas_call x1, Pallas kernels, fused(): pl.pallas_call(functools.partial(kernel, n, factor, width), out_shape=(pl...  56.9 us
    pallas_call x1, Pallas kernels, fused(): pl.pallas_call(write_out, out_shape=(jax.ShapeDtypeStruct((tokens, units)...  2.22 us

profile of v5, /device:TPU:0, one launch (start us, length us, event | category | flops | bytes accessed | tf_op | source)
XLA Modules:
  0.0 59.7 jit_solution(12884577828217020249)
XLA Ops:
  0.6 56.9 %shard_map.75 = (bf16[1024,768]{1,0:T(8,128)(2,1)S(1)}, bf16[1024,768]{1,0:T(8,128)(2,1)S(1)}, f32[16,48,512]{2,1,0:T(8,128)S(1)}, f32[1,768]{1,0:T(1,128)S(1)}) custom-call(bf16[1024,768]{1,0:T(8,128)(2,1)} %g_hbm.1, bf16[1024,768]{1,0:T(8,128)(2,1)} %u_hbm.1, bf16[1024,2048]{1,0:T(8,128)(2,1)} %og_hbm.1, bf16[16,48,512]{2,1,0:T(8,128)(2,1)} %bitcast.3), custom_call_target="tpu_custom_call" | custom-call | tf_op jit(solution)/shard_map/pallas_call | solution.py:538
  57.5 2.2 %shard_map.76 = (bf16[1024,768]{1,0:T(8,128)(2,1)}, bf16[1024,768]{1,0:T(8,128)(2,1)}, f32[768,512]{1,0:T(8,128)}, f32[768]{0:T(1024)}) custom-call(bf16[1024,768]{1,0:T(8,128)(2,1)S(1)} %get-tuple-element.8.dg, bf16[1024,768]{1,0:T(8,128)(2,1)S(1)} %get-tuple-element.9.du, f32[768,512]{1,0:T(8,128)S(1)} %bitcast.2, f32[1,768]{1,0:T(1,128)S(1)} %get-tuple-element.11.en), custom_call_target="tpu_custom_call" | custom-call | tf_op jit(solution)/shard_map/pallas_call | solution.py:588
